TPU v7x, 32 devices: a whole 2x2x4 slice. The times are simulated.
32 devices in a mesh: ep: 32 (over z, y, x, core).
Axes of the slice: x: 2, y: 2, z: 4, core: 2. Of those that a mesh axis runs over, the one named last changes fastest.
Arguments:
- hidden_in: bfloat16 [512, 2048], P('ep'), may hold values from -6 to 6
- lengths: int32 [512], P('ep'), may hold values from 1 to 1024
- attn_gain: float32 [2048], replicated, may hold values from 0.1 to 1.9
- query_weight: bfloat16 [2048, 512], replicated, may hold values from -0.125 to 0.125
- key_weight: bfloat16 [2048, 128], replicated, may hold values from -0.125 to 0.125
- value_weight: bfloat16 [2048, 128], replicated, may hold values from -0.125 to 0.125
- score_bias: float32 [8], replicated, may hold values from -7.5 to -3.5
- out_weight: bfloat16 [512, 2048], replicated, may hold values from -0.25 to 0.25
- key_cache: bfloat16 [512, 1024, 128], P('ep'), may hold values from -6 to 6
- value_cache: bfloat16 [512, 1024, 128], P('ep'), may hold values from -10 to 10
- ffn_gain: float32 [2048], replicated, may hold values from 0.1 to 1.9
- routes: int32 [512, 4], P('ep'), may hold values from 0 to 31, all different within a row; in each aligned block of 16 rows (0 to 15, 16 to 31, ...) at most 2 rows name the same one
- route_weights: float32 [512, 4], P('ep'), may hold values from 0.25 to 1
- expert_gate: bfloat16 [32, 2048, 512], P('ep'), may hold values from -0.125 to 0.125
- expert_up: bfloat16 [32, 2048, 512], P('ep'), may hold values from -0.125 to 0.125
- expert_down: bfloat16 [32, 512, 2048], P('ep'), may hold values from -0.25 to 0.25
- dense_gate: bfloat16 [2048, 2048], P(None, 'ep'), may hold values from -0.125 to 0.125
- dense_up: bfloat16 [2048, 2048], P(None, 'ep'), may hold values from -0.125 to 0.125
- dense_down: bfloat16 [2048, 2048], P(None, 'ep'), may hold values from -0.125 to 0.125
- branch_gate: float32 [2048], replicated, may hold values from -0.125 to 0.125
Outputs:
- hidden_out: bfloat16 [512, 2048], P('ep')
- new_keys: bfloat16 [512, 128], P('ep')
- new_values: bfloat16 [512, 128], P('ep')
Inputs may be any that keep to these rules, and one draw needn't show every extreme that they name: `routes`: in each device's 16 rows no expert is named twice.
All inputs are finite; a program needn't handle non-finite values.
Results may differ from a plain program's by a relative error of at most 0.0061.
Values may be sent and summed in bfloat16 or wider, within the bound.
A program may use at most 128 MiB of HBM per device.

v0:
```python
import functools

import jax
import jax.numpy as jnp
from jax import lax
from jax.experimental import pallas as pl
from jax.experimental.pallas import tpu as pltpu
from jax.sharding import PartitionSpec as P

HEADS = 8
KV_HEADS = 2
HEAD = 64
TOP = 4
EXTRA = 128
SPAN = 256
MESH = pl.DeviceIdType.MESH
F32 = jnp.float32
BF16 = jnp.bfloat16

norm_eps = 1e-06


def rms_norm(as_float, gain):
    scaled = as_float * lax.rsqrt(jnp.mean(as_float * as_float, axis=-1, keepdims=True) + norm_eps)
    return (scaled * gain).astype(BF16)


def three_parts(value):
    high = value.astype(BF16)
    rest = value - high.astype(F32)
    mid = rest.astype(BF16)
    low = (rest - mid.astype(F32)).astype(BF16)
    return high, mid, low


def dot(a, b):
    return jnp.dot(a, b, preferred_element_type=F32)


def dot_t(a, b):
    return lax.dot_general(a, b, (((1,), (1,)), ((), ())), preferred_element_type=F32)


def attend_part(
    prefetch,
    lengths_hbm,
    bias_hbm,
    hidden_hbm,
    attn_gain_hbm,
    ffn_gain_hbm,
    branch_gate_hbm,
    routes_hbm,
    route_weights_hbm,
    query_w,
    key_w,
    value_w,
    out_w,
    key_c,
    value_c,
    middle_out,
    rows_out,
    keys_out,
    values_out,
    wq,
    wk,
    wv,
    wo,
    kbuf,
    vbuf,
    qs,
    zs,
    mix,
    lengths,
    bias,
    hidden,
    attn_gain,
    ffn_gain,
    branch_gate,
    routes,
    route_weights,
    small_sem,
    wsem,
    ksem,
    vsem,
):
    seqs, width = hidden.shape
    cache_len = kbuf.shape[1]
    per_group = HEADS // KV_HEADS
    kv_width = KV_HEADS * HEAD
    small = []
    for src, dst in (
        (hidden_hbm, hidden),
        (attn_gain_hbm, attn_gain),
        (lengths_hbm, lengths),
        (bias_hbm, bias),
        (ffn_gain_hbm, ffn_gain),
        (branch_gate_hbm, branch_gate),
        (routes_hbm, routes),
        (route_weights_hbm, route_weights),
    ):
        small.append(pltpu.make_async_copy(src, dst, small_sem.at[len(small)]))
        small[-1].start()
    copies = []
    for i, (src, dst) in enumerate(((query_w, wq), (key_w, wk), (value_w, wv))):
        copies.append(pltpu.make_async_copy(src, dst, wsem.at[i]))
        copies[-1].start()
    kcopies, vcopies = [], []
    for b in range(seqs):
        kcopies.append(pltpu.make_async_copy(key_c.at[b], kbuf.at[b], ksem.at[b]))
        vcopies.append(pltpu.make_async_copy(value_c.at[b], vbuf.at[b], vsem.at[b]))
        kcopies[-1].start()
        vcopies[-1].start()
    wo_copy = pltpu.make_async_copy(out_w, wo, wsem.at[3])
    wo_copy.start()

    small[0].wait()
    small[1].wait()
    hidden_f = hidden[...].astype(F32)
    normed = rms_norm(hidden_f, attn_gain[...])
    copies[0].wait()
    queries = dot(normed, wq[...]).astype(BF16).astype(F32) * HEAD ** (-0.5)
    lane = lax.broadcasted_iota(jnp.int32, (seqs, kv_width), 1)
    for h in range(HEADS):
        tile = queries[:, (h // 2) * kv_width : (h // 2 + 1) * kv_width]
        if h % 2 != h // per_group:
            tile = pltpu.roll(tile, HEAD, 1)
        qs[:, h, :] = jnp.where(lane // HEAD == h // per_group, tile, 0.0)
    small[2].wait()
    small[3].wait()
    copies[1].wait()
    keys_out[...] = dot(normed, wk[...]).astype(BF16)
    copies[2].wait()
    values_out[...] = dot(normed, wv[...]).astype(BF16)

    pos_r = lax.broadcasted_iota(jnp.int32, (SPAN, SPAN), 0)
    pos_c = lax.broadcasted_iota(jnp.int32, (SPAN, SPAN), 1)
    tri = (pos_r >= pos_c).astype(F32).astype(BF16)
    position = lax.broadcasted_iota(jnp.int32, (HEADS, cache_len), 1)
    head_row = lax.broadcasted_iota(jnp.int32, (HEADS, cache_len), 0)
    head_bias = jnp.zeros((HEADS, cache_len), F32)
    for h in range(HEADS):
        head_bias = jnp.where(head_row == h, bias[h], head_bias)
    group = 8
    spans = cache_len // SPAN
    for g in range(seqs // group):
        keeps = []
        for b in range(g * group, (g + 1) * group):
            kcopies[b].wait()
            z = dot_t(qs[b].astype(BF16), kbuf[b]) + head_bias
            zs[b] = z
            soft = jnp.maximum(z, 0.0) + jnp.log1p(jnp.exp(-jnp.abs(z)))
            keeps.append(jnp.where(position < lengths[b], soft, 0.0))
        parts = three_parts(jnp.concatenate(keeps, axis=0))
        carry = jnp.zeros((group * HEADS, 1), F32)
        suffix = [None] * spans
        for s in reversed(range(spans)):
            cols = slice(s * SPAN, (s + 1) * SPAN)
            inside = dot(parts[0][:, cols], tri) + dot(parts[1][:, cols], tri) + dot(parts[2][:, cols], tri)
            suffix[s] = inside + carry
            carry = carry + inside[:, :1]
        suffix = jnp.concatenate(suffix, axis=1)
        for i, b in enumerate(range(g * group, (g + 1) * group)):
            log_w = zs[b] - suffix[i * HEADS : (i + 1) * HEADS]
            w = jnp.where(position < lengths[b], jnp.exp(log_w), 0.0).astype(BF16)
            vcopies[b].wait()
            mix[b] = dot(w, vbuf[b])
        if g == 0:
            prefetch()
    tiles = []
    for t in range(HEADS // 2):
        pieces = []
        for h in (2 * t, 2 * t + 1):
            tile = mix[:, h, :]
            if h % 2 != h // per_group:
                tile = pltpu.roll(tile, HEAD, 1)
            pieces.append(tile)
        tiles.append(jnp.where(lane < HEAD, pieces[0], pieces[1]))
    attended = jnp.concatenate(tiles, axis=1).astype(BF16)
    wo_copy.wait()
    middle = hidden_f + dot(attended, wo[...])
    middle_out[...] = middle
    for copy in small[4:]:
        copy.wait()
    ffn_in = rms_norm(middle, ffn_gain[...])
    rows_out[:, :width] = ffn_in
    gate = jax.nn.sigmoid(jnp.sum(ffn_in.astype(F32) * branch_gate[...], axis=1, keepdims=True))
    by_row = [routes[...].astype(F32)] + [part.astype(F32) for part in three_parts(route_weights[...])]
    by_row.append(jnp.zeros((EXTRA - 4 * TOP, seqs), F32))
    by_row = jnp.concatenate(by_row, axis=0)
    extra = jnp.concatenate([by_row, jnp.zeros((EXTRA, EXTRA - seqs), F32)], axis=1).T[:seqs]
    extra_lane = lax.broadcasted_iota(jnp.int32, (seqs, EXTRA), 1)
    for i, part in enumerate(three_parts(gate)):
        extra = jnp.where(extra_lane == 4 * TOP + i, part.astype(F32), extra)
    rows_out[:, width:] = extra.astype(BF16)


def flip(v, j):
    if j == 0:
        return v
    if j == 1:
        return v + 1 - 2 * (v % 2)
    if j == 2:
        return (v + 2) % 4
    return 3 - v


def layer_kernel(dims, cap, *refs):
    attend_in, ffn_in, whole, refs = refs[:14], refs[14:20], refs[20], refs[21:]
    width = ffn_in[3].shape[1]
    kv_width = KV_HEADS * HEAD
    outs = [
        whole.at[:, pl.ds(0, width)],
        whole.at[:, pl.ds(width, kv_width)],
        whole.at[:, pl.ds(width + kv_width, kv_width)],
    ]
    attend_scratch, ffn_scratch = refs[:21], refs[21:]

    def attend(prefetch, middle, rows):
        attend_part(prefetch, *attend_in, middle, rows, *outs[1:], *attend_scratch)

    ffn_part(dims, cap, attend, *ffn_in, outs[0], *ffn_scratch)


def ffn_part(
    dims,
    cap,
    attend,
    eg_hbm,
    eu_hbm,
    ed_hbm,
    dg_hbm,
    du_hbm,
    dd_hbm,
    out,
    middle,
    rows,
    eg,
    eu,
    ed,
    dg,
    du,
    dd,
    buf,
    part,
    rcore,
    summed,
    rx,
    ry,
    qa,
    qb,
    rya,
    rxb,
    tsum,
    rz,
    wsem,
    s_sem,
    r_sem,
):
    C, Z, Y, X = dims
    seqs, width = middle.shape
    half = width // 2
    me = lax.axis_index("ep")
    c = me % C
    x = (me // C) % X
    y = (me // (C * X)) % Y
    z = me // (C * X * Y)

    def dev(zz, yy, xx, cc):
        return (((zz * Y + yy) * X + xx) * C + cc,)

    z_mates = [dev(flip(z, j), y, x, c) for j in range(1, Z)]
    y_mates = [dev(z, flip(y, o), x, c) for o in range(1, Y)]
    x_mates = [dev(z, y, flip(x, o), c) for o in range(1, X)]
    peer = dev(z, y, x, 1 - c)
    barrier = pltpu.get_barrier_semaphore()
    mates = z_mates + y_mates + x_mates + [peer]
    for mate in mates:
        pl.semaphore_signal(barrier, inc=1, device_id=mate, device_id_type=MESH)
    weight_copies = []

    def prefetch():
        for i, (src, dst) in enumerate(
            ((dg_hbm, dg), (du_hbm, du), (eg_hbm, eg), (eu_hbm, eu), (ed_hbm, ed), (dd_hbm, dd))
        ):
            weight_copies.append(pltpu.make_async_copy(src, dst, wsem.at[i]))
            weight_copies[-1].start()

    attend(prefetch, middle, rows)
    pl.semaphore_wait(barrier, len(mates))

    sent = []
    count = [0]

    def send(src, dst, where):
        k = count[0]
        count[0] += 1
        copy = pltpu.make_async_remote_copy(
            src_ref=src,
            dst_ref=dst,
            send_sem=s_sem.at[k],
            recv_sem=r_sem.at[k],
            device_id=where,
            device_id_type=MESH,
        )
        copy.start()
        sent.append(copy)
        return copy

    A = pl.ds(0, half)
    B = pl.ds(half, width + EXTRA - half)
    B_out = pl.ds(half, width - half)
    z_copies = {}
    for j in range(1, Z):
        z_copies[j] = send(rows, buf.at[c, z, y, x], z_mates[j - 1])
    buf[c, z, y, x] = rows[...]

    blocks = C * Y * X
    group_rows = blocks * seqs
    state = [dict() for _ in range(Z)]

    def spread_first(j):
        zj = flip(z, j)
        if j:
            z_copies[j].wait_recv()
        src = buf.at[c, zj, y, x] if j else rows
        state[j]["y"] = [send(src.at[:, A], buf.at[c, zj, y, x, :, A], mate) for mate in y_mates]
        state[j]["x"] = [send(src.at[:, B], buf.at[c, zj, y, x, :, B], mate) for mate in x_mates]

    def spread_second(j):
        zj = flip(z, j)
        for copy in state[j]["y"]:
            copy.wait_recv()
        spot = buf.at[c, zj, :, x, :, A]
        xs = [send(spot, spot, mate) for mate in x_mates]
        for copy in state[j]["x"]:
            copy.wait_recv()
        spot = buf.at[c, zj, y, :, :, B]
        state[j]["second"] = xs + [send(spot, spot, mate) for mate in y_mates]

    def spread_core(j):
        zj = flip(z, j)
        for copy in state[j]["second"]:
            copy.wait_recv()
        spot = buf.at[c, zj]
        state[j]["core"] = send(spot, spot, peer)

    row_i = lax.broadcasted_iota(jnp.int32, (group_rows, group_rows), 0)
    col_i = lax.broadcasted_iota(jnp.int32, (group_rows, group_rows), 1)
    earlier = ((row_i // seqs == col_i // seqs) & (row_i < col_i)).astype(F32).astype(BF16)
    slots = blocks * cap
    slot_i = lax.broadcasted_iota(jnp.int32, (slots, group_rows), 0)
    slot_block = lax.broadcasted_iota(jnp.int32, (slots, group_rows), 1) // seqs

    def compute(j):
        zj = flip(z, j)
        state[j]["core"].wait_recv()
        got = buf[:, zj].reshape(group_rows, width + EXTRA)
        tokens = got[:, :width]
        extra = got[:, width:].astype(F32)
        gate = extra[:, 4 * TOP : 4 * TOP + 1] + extra[:, 4 * TOP + 1 : 4 * TOP + 2] + extra[:, 4 * TOP + 2 : 4 * TOP + 3]
        flat = extra.T
        if j == 0:
            weight_copies[0].wait()
            weight_copies[1].wait()
        dense_gate = dot_t(tokens, dg[...])
        dense_up = dot_t(tokens, du[...])
        dense = (dense_gate / (1.0 + jnp.exp(-dense_gate)) * dense_up * gate).astype(BF16)
        hit = (flat[0:TOP] == me.astype(F32)).astype(F32)
        weight = flat[TOP : 2 * TOP] + flat[2 * TOP : 3 * TOP] + flat[3 * TOP : 4 * TOP]
        named = jnp.sum(hit, axis=0, keepdims=True)
        row_weight = jnp.sum(hit * weight, axis=0, keepdims=True)
        ranks = dot(jnp.broadcast_to(named, (16, group_rows)).astype(BF16), earlier)[0:1]
        slot = slot_block * cap + ranks.astype(jnp.int32)
        pick = jnp.where((slot == slot_i) & (named > 0.0), 1.0, 0.0)
        slot_weight = jnp.sum(pick * row_weight, axis=1, keepdims=True)
        pick = pick.astype(BF16)
        picked = dot(pick, tokens).astype(BF16)
        if j == 0:
            weight_copies[2].wait()
            weight_copies[3].wait()
        gate_pre = dot(picked, eg[0])
        up_pre = dot(picked, eu[0])
        act = (gate_pre / (1.0 + jnp.exp(-gate_pre)) * up_pre).astype(BF16)
        if j == 0:
            weight_copies[4].wait()
            weight_copies[5].wait()
        expert = dot(act, ed[0]).astype(BF16).astype(F32)
        expert = (expert * slot_weight).astype(BF16)
        total = dot(dense, dd[...]) + lax.dot_general(
            pick, expert, (((0,), (0,)), ((), ())), preferred_element_type=F32
        )
        part[:, j] = total.astype(BF16).reshape(C, Y, X, seqs, width)
        state[j]["rc"] = send(part.at[1 - c, j], rcore.at[j], peer)

    def reduce_core(j):
        state[j]["rc"].wait_recv()
        summed[j] = (part[c, j].astype(F32) + rcore[j].astype(F32)).astype(BF16)
        state[j]["rx"] = [
            send(summed.at[j, :, flip(x, o), :, A], rx.at[j, o - 1], x_mates[o - 1]) for o in range(1, X)
        ]
        state[j]["ry"] = [
            send(summed.at[j, flip(y, o), :, :, B_out], ry.at[j, o - 1], y_mates[o - 1]) for o in range(1, Y)
        ]

    def reduce_first(j):
        total = summed[j, :, x, :, :half].astype(F32)
        for o, copy in enumerate(state[j]["rx"]):
            copy.wait_recv()
            total = total + rx[j, o].astype(F32)
        qa[j] = total.astype(BF16)
        state[j]["rya"] = [send(qa.at[j, flip(y, o)], rya.at[j, o - 1], y_mates[o - 1]) for o in range(1, Y)]
        total = summed[j, y, :, :, half:].astype(F32)
        for o, copy in enumerate(state[j]["ry"]):
            copy.wait_recv()
            total = total + ry[j, o].astype(F32)
        qb[j] = total.astype(BF16)
        state[j]["rxb"] = [send(qb.at[j, flip(x, o)], rxb.at[j, o - 1], x_mates[o - 1]) for o in range(1, X)]

    def reduce_second(j):
        total_a = qa[j, y].astype(F32)
        for o, copy in enumerate(state[j]["rya"]):
            copy.wait_recv()
            total_a = total_a + rya[j, o].astype(F32)
        total_b = qb[j, x].astype(F32)
        for o, copy in enumerate(state[j]["rxb"]):
            copy.wait_recv()
            total_b = total_b + rxb[j, o].astype(F32)
        if j:
            tsum[j, :, :half] = total_a.astype(BF16)
            tsum[j, :, half:] = total_b.astype(BF16)
            state[j]["z"] = send(tsum.at[j], rz.at[j], z_mates[j - 1])
        else:
            state[j]["own"] = (total_a, total_b)

    stages = (spread_first, spread_second, spread_core, compute, reduce_core, reduce_first, reduce_second)
    order = list(range(Z))
    for t in range(len(stages) + Z - 1):
        for s, stage in enumerate(stages):
            if 0 <= t - s < Z:
                stage(order[t - s])
    total_a, total_b = state[0]["own"]
    total_a = total_a + middle[:, :half]
    total_b = total_b + middle[:, half:]
    for j in range(1, Z):
        state[j]["z"].wait_recv()
        total_a = total_a + rz[j, :, :half].astype(F32)
        total_b = total_b + rz[j, :, half:].astype(F32)
    out[:, :half] = total_a.astype(BF16)
    out[:, half:] = total_b.astype(BF16)
    for copy in sent:
        copy.wait_send()


def grid_of(devices):
    cores = 2
    rest = devices // cores
    z = min(rest, 4)
    rest //= z
    x = 1
    while x * x < rest:
        x *= 2
    return cores, z, rest // x, x


def per_device(
    hidden_in,
    lengths,
    attn_gain,
    query_weight,
    key_weight,
    value_weight,
    score_bias,
    out_weight,
    key_cache,
    value_cache,
    ffn_gain,
    routes,
    route_weights,
    expert_gate,
    expert_up,
    expert_down,
    dense_gate,
    dense_up,
    dense_down,
    branch_gate,
    *,
    devices,
):
    seqs, width = hidden_in.shape
    cache_len, kv_width = key_cache.shape[1:]
    vmem = pl.BlockSpec(memory_space=pltpu.VMEM)
    hbm = pl.BlockSpec(memory_space=pltpu.HBM)
    sds = jax.ShapeDtypeStruct
    dma = pltpu.SemaphoreType.DMA
    attend_scratch = [
        pltpu.VMEM(query_weight.shape, BF16),
        pltpu.VMEM(key_weight.shape, BF16),
        pltpu.VMEM(value_weight.shape, BF16),
        pltpu.VMEM(out_weight.shape, BF16),
        pltpu.VMEM(key_cache.shape, BF16),
        pltpu.VMEM(value_cache.shape, BF16),
        pltpu.VMEM((seqs, HEADS, kv_width), F32),
        pltpu.VMEM((seqs, HEADS, cache_len), F32),
        pltpu.VMEM((seqs, HEADS, kv_width), F32),
        pltpu.SMEM((seqs,), jnp.int32),
        pltpu.SMEM((HEADS,), F32),
        pltpu.VMEM((seqs, width), BF16),
        pltpu.VMEM((1, width), F32),
        pltpu.VMEM((1, width), F32),
        pltpu.VMEM((1, width), F32),
        pltpu.VMEM((TOP, seqs), jnp.int32),
        pltpu.VMEM((TOP, seqs), F32),
        dma((8,)),
        dma((4,)),
        dma((seqs,)),
        dma((seqs,)),
    ]
    dense_gate, dense_up, dense_down = dense_gate.T, dense_up.T, dense_down.T
    dims = grid_of(devices)
    C, Z, Y, X = dims
    half = width // 2
    cap = max(1, seqs * TOP // (expert_gate.shape[0] * devices))
    copies = (Z - 1) * 2 + Z * (4 * (X - 1) + 4 * (Y - 1) + 2)
    scratch = [
        expert_gate.shape,
        expert_up.shape,
        expert_down.shape,
        dense_gate.shape,
        dense_up.shape,
        dense_down.shape,
        (C, Z, Y, X, seqs, width + EXTRA),
        (C, Z, Y, X, seqs, width),
        (Z, Y, X, seqs, width),
        (Z, Y, X, seqs, width),
        (Z, max(X - 1, 1), Y, seqs, half),
        (Z, max(Y - 1, 1), X, seqs, width - half),
        (Z, Y, seqs, half),
        (Z, X, seqs, width - half),
        (Z, max(Y - 1, 1), seqs, half),
        (Z, max(X - 1, 1), seqs, width - half),
        (Z, seqs, width),
        (Z, seqs, width),
    ]
    whole = pl.pallas_call(
        functools.partial(layer_kernel, dims, cap),
        out_shape=sds((seqs, width + 2 * kv_width), BF16),
        in_specs=[hbm] * 20,
        out_specs=vmem,
        scratch_shapes=attend_scratch
        + [pltpu.VMEM((seqs, width), F32), pltpu.VMEM((seqs, width + EXTRA), BF16)]
        + [pltpu.VMEM(shape, BF16) for shape in scratch]
        + [dma((6,)), dma((copies,)), dma((copies,))],
        compiler_params=pltpu.CompilerParams(
            collective_id=0,
            has_side_effects=True,
            vmem_limit_bytes=67043328,
        ),
        name="layer",
    )(
        lengths,
        score_bias,
        hidden_in,
        attn_gain.reshape(1, width),
        ffn_gain.reshape(1, width),
        branch_gate.reshape(1, width),
        routes.T,
        route_weights.T,
        query_weight,
        key_weight,
        value_weight,
        out_weight,
        key_cache,
        value_cache,
        expert_gate,
        expert_up,
        expert_down,
        dense_gate,
        dense_up,
        dense_down,
    )
    return whole[:, :width], whole[:, width : width + kv_width], whole[:, width + kv_width :]


def solution(mesh):
    return jax.shard_map(
        functools.partial(per_device, devices=mesh.shape["ep"]),
        mesh=mesh,
        in_specs=(
            P("ep", None),
            P("ep"),
            P(),
            P(),
            P(),
            P(),
            P(),
            P(),
            P("ep", None, None),
            P("ep", None, None),
            P(),
            P("ep", None),
            P("ep", None),
            P("ep", None, None),
            P("ep", None, None),
            P("ep", None, None),
            P(None, "ep"),
            P(None, "ep"),
            P(None, "ep"),
            P(),
        ),
        out_specs=(P("ep", None), P("ep", None), P("ep", None)),
        check_vma=False,
    )
```

profile of v0, /device:TPU:0, one launch (start us, length us, event | category | flops | bytes accessed | tf_op | source)
XLA Modules:
  0.0 54.5 jit_solution(4662784252492329081)
XLA Ops:
  0.6 51.1 %layer.1 = bf16[16,2304]{1,0:T(8,128)(2,1)} custom-call(s32[16]{0:T(128)} %refs_0_.1, f32[8]{0:T(128)} %refs_1_.1, bf16[16,2048]{1,0:T(8,128)(2,1)} %refs_2_.1, f32[1,2048]{1,0:T(1,128)} %bitcast.11, f32[1,2048]{1,0:T(1,128)} %bitcast.12, f32[1,2048]{1,0:T(1,128)} %bitcast.13, s32[4,16]{1,0:T(4,128)} %bitcast.14, f32[4,16]{1,0:T(4,128)} %bitcast.15, ...), custom_call_target="tpu_custom_call" | custom-call | tf_op jit(solution)/shard_map/layer/pallas_call | solution.py:544
  51.7 1.3 %fusion = (bf16[16,128]{1,0:T(8,128)(2,1)}, bf16[16,128]{1,0:T(8,128)(2,1)}) fusion(bf16[16,2304]{1,0:T(8,128)(2,1)} %layer.1), kind=kLoop, calls=%fused_computation | loop fusion | bytes 16384 | tf_op jit(solution)/shard_map/slice | solution.py:581
  53.0 1.5 %slice.9 = bf16[16,2048]{1,0:T(8,128)(2,1)} slice(bf16[16,2304]{1,0:T(8,128)(2,1)} %layer.1), slice={[0:16], [0:2048]} | slice | bytes 131072 | tf_op jit(solution)/shard_map/slice | solution.py:581
where the time goes:
time: 54.6 us; the launch traced here: 54.5 us
  Pallas kernels  51.1 us (94%)
  local copies, waits for them, and re-layouts  2.76 us (5%)
  between operations  0.65 us (1%)
    pallas_call x1, Pallas kernels, per_device(): pl.pallas_call(functools.partial(layer_kernel, dims, cap), out_shape=sds(...  51.1 us
    slice x1, local copies, waits for them, and re-layouts, per_device(): whole[:, :width]  1.47 us
    slice x1, local copies, waits for them, and re-layouts, per_device(): whole[:, width + kv_width:]  1.28 us

commit v1 on v0

--- a/solution.py
+++ b/solution.py
@@ -13,6 +13,7 @@
 TOP = 4
 EXTRA = 128
 SPAN = 256
+GROUP = 8
 MESH = pl.DeviceIdType.MESH
 F32 = jnp.float32
 BF16 = jnp.bfloat16
@@ -103,21 +104,33 @@
     copies = []
     for i, (src, dst) in enumerate(((query_w, wq), (key_w, wk), (value_w, wv))):
         copies.append(pltpu.make_async_copy(src, dst, wsem.at[i]))
-        copies[-1].start()
+    group = min(GROUP, seqs)
+    groups = seqs // group
     kcopies, vcopies = [], []
-    for b in range(seqs):
-        kcopies.append(pltpu.make_async_copy(key_c.at[b], kbuf.at[b], ksem.at[b]))
-        vcopies.append(pltpu.make_async_copy(value_c.at[b], vbuf.at[b], vsem.at[b]))
-        kcopies[-1].start()
-        vcopies[-1].start()
+    for b in range(seqs // 2):
+        pair = pl.ds(2 * b, 2)
+        kcopies.append(pltpu.make_async_copy(key_c.at[pair], kbuf.at[pair], ksem.at[b]))
+        vcopies.append(pltpu.make_async_copy(value_c.at[pair], vbuf.at[pair], vsem.at[b]))
     wo_copy = pltpu.make_async_copy(out_w, wo, wsem.at[3])
-    wo_copy.start()
-
+
+    def fetch(g):
+        for copy in kcopies[g * group // 2 : (g + 1) * group // 2]:
+            copy.start()
+        for copy in vcopies[g * group // 2 : (g + 1) * group // 2]:
+            copy.start()
+
+    copies[0].start()
+    fetch(0)
     small[0].wait()
     small[1].wait()
     hidden_f = hidden[...].astype(F32)
     normed = rms_norm(hidden_f, attn_gain[...])
     copies[0].wait()
+    for g in range(1, groups):
+        fetch(g)
+    wo_copy.start()
+    copies[1].start()
+    copies[2].start()
     queries = dot(normed, wq[...]).astype(BF16).astype(F32) * HEAD ** (-0.5)
     lane = lax.broadcasted_iota(jnp.int32, (seqs, kv_width), 1)
     for h in range(HEADS):
@@ -127,10 +140,6 @@
         qs[:, h, :] = jnp.where(lane // HEAD == h // per_group, tile, 0.0)
     small[2].wait()
     small[3].wait()
-    copies[1].wait()
-    keys_out[...] = dot(normed, wk[...]).astype(BF16)
-    copies[2].wait()
-    values_out[...] = dot(normed, wv[...]).astype(BF16)
 
     pos_r = lax.broadcasted_iota(jnp.int32, (SPAN, SPAN), 0)
     pos_c = lax.broadcasted_iota(jnp.int32, (SPAN, SPAN), 1)
@@ -140,32 +149,50 @@
     head_bias = jnp.zeros((HEADS, cache_len), F32)
     for h in range(HEADS):
         head_bias = jnp.where(head_row == h, bias[h], head_bias)
-    group = 8
     spans = cache_len // SPAN
-    for g in range(seqs // group):
+    blank = jnp.zeros((HEADS, kv_width), F32)
+    for g in range(groups):
+        members = range(g * group, (g + 1) * group)
+        for b in members[::2]:
+            kcopies[b // 2].wait()
         keeps = []
-        for b in range(g * group, (g + 1) * group):
-            kcopies[b].wait()
-            z = dot_t(qs[b].astype(BF16), kbuf[b]) + head_bias
-            zs[b] = z
-            soft = jnp.maximum(z, 0.0) + jnp.log1p(jnp.exp(-jnp.abs(z)))
-            keeps.append(jnp.where(position < lengths[b], soft, 0.0))
-        parts = three_parts(jnp.concatenate(keeps, axis=0))
-        carry = jnp.zeros((group * HEADS, 1), F32)
+        for b in members[::2]:
+            both = jnp.concatenate(
+                [jnp.concatenate([qs[b], blank], axis=1), jnp.concatenate([blank, qs[b + 1]], axis=1)], axis=0
+            ).astype(BF16)
+            scores = dot_t(both, jnp.concatenate([kbuf[b], kbuf[b + 1]], axis=1))
+            for i in range(2):
+                z = scores[i * HEADS : (i + 1) * HEADS] + head_bias
+                zs[b + i] = z
+                soft = jnp.maximum(z, 0.0) + jnp.log(1.0 + jnp.exp(-jnp.abs(z)))
+                keeps.append(jnp.where(position < lengths[b + i], soft, 0.0))
+        parts = jnp.concatenate(three_parts(jnp.concatenate(keeps, axis=0)), axis=0)
+        rows = group * HEADS
+        carry = jnp.zeros((rows, 1), F32)
         suffix = [None] * spans
         for s in reversed(range(spans)):
-            cols = slice(s * SPAN, (s + 1) * SPAN)
-            inside = dot(parts[0][:, cols], tri) + dot(parts[1][:, cols], tri) + dot(parts[2][:, cols], tri)
+            sums = dot(parts[:, s * SPAN : (s + 1) * SPAN], tri)
+            inside = sums[:rows] + sums[rows : 2 * rows] + sums[2 * rows :]
             suffix[s] = inside + carry
             carry = carry + inside[:, :1]
         suffix = jnp.concatenate(suffix, axis=1)
-        for i, b in enumerate(range(g * group, (g + 1) * group)):
+        ws = []
+        for i, b in enumerate(members):
             log_w = zs[b] - suffix[i * HEADS : (i + 1) * HEADS]
-            w = jnp.where(position < lengths[b], jnp.exp(log_w), 0.0).astype(BF16)
-            vcopies[b].wait()
-            mix[b] = dot(w, vbuf[b])
+            ws.append(jnp.where(position < lengths[b], jnp.exp(log_w), 0.0))
+        for b in members[::2]:
+            vcopies[b // 2].wait()
+        for i, b in enumerate(members[::2]):
+            both = jnp.concatenate(ws[2 * i : 2 * i + 2], axis=0).astype(BF16)
+            mixed = dot(both, jnp.concatenate([vbuf[b], vbuf[b + 1]], axis=1))
+            mix[b] = mixed[:HEADS, :kv_width]
+            mix[b + 1] = mixed[HEADS:, kv_width:]
         if g == 0:
             prefetch()
+    copies[1].wait()
+    keys_out[...] = dot(normed, wk[...]).astype(BF16)
+    copies[2].wait()
+    values_out[...] = dot(normed, wv[...]).astype(BF16)
     tiles = []
     for t in range(HEADS // 2):
         pieces = []
@@ -449,6 +476,18 @@
     out[:, half:] = total_b.astype(BF16)
     for copy in sent:
         copy.wait_send()
+
+
+def split_kernel(whole, *refs):
+    outs, sem = refs[:-1], refs[-1]
+    copies, start = [], 0
+    for i, out in enumerate(outs):
+        size = out.shape[1]
+        copies.append(pltpu.make_async_copy(whole.at[:, pl.ds(start, size)], out, sem.at[i]))
+        copies[-1].start()
+        start += size
+    for copy in copies:
+        copy.wait()
 
 
 def grid_of(devices):
@@ -543,7 +582,7 @@
     ]
     whole = pl.pallas_call(
         functools.partial(layer_kernel, dims, cap),
-        out_shape=sds((seqs, width + 2 * kv_width), BF16),
+        out_shape=pltpu.VMEM((seqs, width + 2 * kv_width), BF16),
         in_specs=[hbm] * 20,
         out_specs=vmem,
         scratch_shapes=attend_scratch
@@ -553,7 +592,7 @@
         compiler_params=pltpu.CompilerParams(
             collective_id=0,
             has_side_effects=True,
-            vmem_limit_bytes=67043328,
+            vmem_limit_bytes=62914560,
         ),
         name="layer",
     )(
@@ -578,7 +617,16 @@
         dense_up,
         dense_down,
     )
-    return whole[:, :width], whole[:, width : width + kv_width], whole[:, width + kv_width :]
+    return tuple(
+        pl.pallas_call(
+            split_kernel,
+            out_shape=[sds((seqs, size), BF16) for size in (width, kv_width, kv_width)],
+            in_specs=[vmem],
+            out_specs=[hbm] * 3,
+            scratch_shapes=[dma((3,))],
+            name="split",
+        )(pltpu.with_memory_space_constraint(whole, pltpu.VMEM))
+    )
 
 
 def solution(mesh):

time: 54.6 us -> 47.9 us (0.88)
  Pallas kernels: 51.1 us -> 47.1 us
  local copies, waits for them, and re-layouts: 2.76 us -> 0 us
    pallas_call x1 -> x2, Pallas kernels: 51.1 us -> 47.1 us  [the longest x1 46.5 us: per_device(): pl.pallas_call(functools.partial(layer_kernel, dims, cap), out_shape=pltp...]
    slice x2 -> x0, local copies, waits for them, and re-layouts: 2.76 us -> none  [the longest x1 1.47 us: per_device(): whole[:, :width]]
where the time goes in v1:
time: 47.9 us; the launch traced here: 47.8 us
  Pallas kernels  47.1 us (98%)
  between operations  0.65 us (1%)
    pallas_call x1, Pallas kernels, per_device(): pl.pallas_call(functools.partial(layer_kernel, dims, cap), out_shape=pltp...  46.5 us

profile of v1, /device:TPU:0, one launch (start us, length us, event | category | flops | bytes accessed | tf_op | source)
XLA Modules:
  0.0 47.8 jit_solution(18238015524339304363)
XLA Ops:
  0.6 46.5 %layer.1.whole = bf16[16,2304]{1,0:T(8,128)(2,1)S(1)} custom-call(s32[16]{0:T(128)} %refs_0_.1, f32[8]{0:T(128)} %refs_1_.1, bf16[16,2048]{1,0:T(8,128)(2,1)} %refs_2_.1, f32[1,2048]{1,0:T(1,128)} %bitcast.11, f32[1,2048]{1,0:T(1,128)} %bitcast.12, f32[1,2048]{1,0:T(1,128)} %bitcast.13, s32[4,16]{1,0:T(4,128)} %bitcast.14, f32[4,16]{1,0:T(4,128)} %bitcast.15, ...), custom_call_target="tpu_custom_call" | custom-call | tf_op jit(solution)/shard_map/layer/pallas_call | solution.py:583
  47.1 0.7 %split.1 = (bf16[16,2048]{1,0:T(8,128)(2,1)}, bf16[16,128]{1,0:T(8,128)(2,1)}, bf16[16,128]{1,0:T(8,128)(2,1)}) custom-call(bf16[16,2304]{1,0:T(8,128)(2,1)S(1)} %layer.1.whole), custom_call_target="tpu_custom_call" | custom-call | tf_op jit(solution)/shard_map/split/pallas_call | solution.py:621
